TPU v7x, 512 devices: a whole 4x8x8 slice. The times are simulated.
512 devices in a mesh: sp: 32 (over z, x), tp: 16 (over y, core).
Axes of the slice: x: 4, y: 8, z: 8, core: 2. Of those that a mesh axis runs over, the one named last changes fastest.
Arguments:
- residual: bfloat16 [8192, 2048], P('sp', 'tp'), may hold values from -26 to 26
- queries: bfloat16 [2048, 8192], P('tp', 'sp'), may hold values from -6 to 6
- keys: bfloat16 [2048, 8192], P('tp', 'sp'), may hold values from -6 to 6
- values: bfloat16 [2048, 8192], P('tp', 'sp'), may hold values from -12 to 12
- forget_cache: float32 [32, 8192], P('tp', 'sp'), as said below
- out_weight: bfloat16 [2048, 2048], P('tp'), may hold values from -0.125 to 0.125
- norm_gain: float32 [2048], replicated, may hold values from 0.1 to 1.9
- routes: int32 [8192, 2], P('sp'), may hold values from 0 to 31, all different within a row; in each aligned block of 256 rows (0 to 255, 256 to 511, ...) at most 20 rows name the same one
- route_weight: float32 [8192, 2], P('sp'), may hold values from 0.2 to 1
- gate_weight: bfloat16 [32, 2048, 4096], P('sp', None, 'tp'), may hold values from -0.125 to 0.125
- up_weight: bfloat16 [32, 2048, 4096], P('sp', None, 'tp'), may hold values from -0.125 to 0.125
- down_weight: bfloat16 [32, 4096, 2048], P('sp', 'tp'), may hold values from -0.09375 to 0.09375
Outputs:
- updated: bfloat16 [8192, 2048], P('sp', 'tp')
Inputs may be any that keep to these rules, and one draw needn't show every extreme that they name: `routes`: each row names 2 different experts; within the 256 rows of one index of sp no expert is named by more than 20 rows, and in the rows of some index some expert is named by exactly 20. `forget_cache`: each head's row never rises from one position to the next.
All inputs are finite; a program needn't handle non-finite values.
Results may differ from a plain program's by a relative error of at most 0.013.
Values may be sent and summed in bfloat16 or wider, within the bound.
No kernel may reach another device: no remote copies, remote signals or barrier semaphores. Data moves between devices by JAX's collectives and lax.ppermute only.
A program may use at most 64 MiB of HBM per device.

v0:
```python
import jax
import jax.numpy as jnp
from jax import lax
from jax.sharding import Mesh
from jax.sharding import PartitionSpec as P

SP = ("sp_0", "sp_1")
norm_eps = 1e-06
masked_score = -1e30
key_span = 1024


def gathered_by_axis(shard, axes, dim):
    out = shard
    for number in range(len(axes) - 1, -1, -1):
        out = lax.all_gather(out, axes[number], axis=dim, tiled=True)
    return out


def cut_along(shard, dim, peers):
    before, after = (shard.shape[:dim], shard.shape[dim + 1 :])
    return jnp.moveaxis(shard.reshape(*before, peers, -1, *after), dim, 0)


def sum_at_owner(shard, axis, dim):
    peers = lax.axis_size(axis)
    pieces = lax.all_to_all(cut_along(shard, dim, peers), axis, 0, 0, tiled=True)
    return jnp.sum(pieces.astype(jnp.float32), axis=0)


def sent_to_all(shard, axis):
    copies = jnp.broadcast_to(shard, (lax.axis_size(axis), *shard.shape))
    return lax.all_to_all(copies, axis, split_axis=0, concat_axis=0, tiled=True)


def taken_together(shard, axis):
    return sent_to_all(shard, axis).sum(axis=0)


def shards(
    residual,
    queries,
    keys,
    values,
    forget_cache,
    out_weight,
    norm_gain,
    routes,
    route_weight,
    gate_weight,
    up_weight,
    down_weight,
):
    sp_count = lax.axis_size(SP)
    token_count, local_width = residual.shape
    model_width = norm_gain.shape[0]
    head_count = forget_cache.shape[0]
    head_width = queries.shape[0] // head_count
    first_token = lax.axis_index(SP) * token_count
    last_token = first_token + token_count - 1
    query_heads = queries.reshape(head_count, head_width, token_count)
    query_place = first_token + jnp.arange(token_count, dtype=jnp.int32)
    score_scale = head_width ** (-0.5)

    def attend_block(state_now, key_block, value_block, cache_block, key_first):
        running_peak, running_total, running_sum = state_now
        block_length = key_block.shape[1]
        key_heads = key_block.reshape(head_count, head_width, block_length)
        value_heads = value_block.reshape(head_count, head_width, block_length)
        scores = (
            jnp.einsum("hdq,hdk->hqk", query_heads, key_heads, preferred_element_type=jnp.float32)
            * score_scale
        )
        scores = scores + forget_cache[:, :, None] - cache_block[:, None, :]
        key_place = key_first + jnp.arange(block_length, dtype=jnp.int32)
        allowed = key_place[None, :] <= query_place[:, None]
        scores = jnp.where(allowed[None], scores, masked_score)
        new_peak = jnp.maximum(running_peak, jnp.max(scores, axis=2))
        weights = jnp.exp(scores - new_peak[:, :, None])
        shrink = jnp.exp(running_peak - new_peak)
        new_total = running_total * shrink + jnp.sum(weights, axis=2)
        new_sum = running_sum * shrink[:, None, :] + jnp.einsum(
            "hdk,hqk->hdq",
            value_heads,
            weights.astype(jnp.bfloat16),
            preferred_element_type=jnp.float32,
        )
        return (new_peak, new_total, new_sum)

    initial = (
        jnp.full((head_count, token_count), masked_score, jnp.float32),
        jnp.zeros((head_count, token_count), jnp.float32),
        jnp.zeros((head_count, head_width, token_count), jnp.float32),
    )
    key_part = gathered_by_axis(keys.astype(jnp.float32), SP, 1).astype(jnp.bfloat16)
    value_part = gathered_by_axis(values.astype(jnp.float32), SP, 1).astype(jnp.bfloat16)
    cache_part = gathered_by_axis(forget_cache, SP, 1)
    part_length = key_part.shape[1]
    block_length = key_span

    def one_block(block_index, state_in):
        start_column = block_index * block_length
        key_block = lax.dynamic_slice_in_dim(key_part, start_column, block_length, 1)
        value_block = lax.dynamic_slice_in_dim(value_part, start_column, block_length, 1)
        cache_block = lax.dynamic_slice_in_dim(cache_part, start_column, block_length, 1)
        return lax.cond(
            start_column <= last_token,
            lambda inner: attend_block(inner, key_block, value_block, cache_block, start_column),
            lambda inner: inner,
            state_in,
        )

    final_peak, final_total, final_sum = lax.fori_loop(
        0, part_length // block_length, one_block, initial
    )
    attended = (
        (final_sum / final_total[:, None, :])
        .astype(jnp.bfloat16)
        .reshape(head_count * head_width, token_count)
    )
    projected = lax.dot_general(
        attended, out_weight, (((0,), (0,)), ((), ())), preferred_element_type=jnp.float32
    )
    head_sum = sum_at_owner(projected.astype(jnp.bfloat16), "tp", 1)
    stream = (residual.astype(jnp.float32) + head_sum).astype(jnp.bfloat16)
    top_count = routes.shape[1]
    item_count = token_count * top_count
    capacity = max(2, token_count * top_count * 5 // (4 * sp_count))
    expert_of = routes.reshape(item_count)
    onehot = (expert_of[:, None] == jnp.arange(sp_count, dtype=jnp.int32)[None, :]).astype(
        jnp.int32
    )
    earlier = jnp.cumsum(onehot, axis=0) - onehot
    target = expert_of * capacity + jnp.sum(earlier * onehot, axis=1)
    matches = target[None, :] == jnp.arange(sp_count * capacity, dtype=jnp.int32)[:, None]
    filled = jnp.any(matches, axis=1)
    source_row = (
        jnp.sum(jnp.where(matches, jnp.arange(item_count, dtype=jnp.int32)[None, :], 0), axis=1)
        // top_count
    )
    local_rows = stream.astype(jnp.float32)
    squares = taken_together(jnp.sum(local_rows * local_rows, axis=1), "tp")
    row_scale = lax.rsqrt(squares / model_width + norm_eps)
    local_gain = lax.dynamic_slice_in_dim(
        norm_gain, lax.axis_index("tp") * local_width, local_width
    )
    normed = (local_rows * row_scale[:, None] * local_gain[None, :]).astype(jnp.bfloat16)
    taken_rows = jnp.take(normed, source_row, axis=0)
    taken_rows = jnp.where(filled[:, None], taken_rows, jnp.zeros((), normed.dtype))
    arrived = lax.all_gather(
        lax.all_to_all(
            taken_rows.reshape(sp_count, capacity, normed.shape[1]),
            SP,
            split_axis=0,
            concat_axis=0,
            tiled=True,
        ),
        "tp",
        axis=2,
        tiled=True,
    )
    source_count = arrived.shape[0]
    slot_count = arrived.shape[1]
    flat_rows = arrived.reshape(source_count * slot_count, model_width)
    gate_value = jnp.dot(flat_rows, gate_weight[0], preferred_element_type=jnp.float32)
    up_value = jnp.dot(flat_rows, up_weight[0], preferred_element_type=jnp.float32)
    hidden = (jax.nn.silu(gate_value) * up_value).astype(jnp.bfloat16)
    down_value = jnp.dot(hidden, down_weight[0], preferred_element_type=jnp.float32)
    summed = sum_at_owner(
        down_value.reshape(source_count, slot_count, model_width).astype(jnp.bfloat16), "tp", 2
    )
    expert_back = lax.all_to_all(
        summed.astype(jnp.bfloat16), SP, split_axis=0, concat_axis=0, tiled=True
    )
    back_rows = expert_back.reshape(sp_count * capacity, local_width)
    picked = (
        jnp.take(back_rows, target, axis=0).astype(jnp.float32)
        * route_weight.reshape(item_count)[:, None]
    )
    mixture = jnp.sum(picked.reshape(token_count, top_count, local_width), axis=1)
    return (stream.astype(jnp.float32) + mixture).astype(jnp.bfloat16)


def solution(mesh):
    finer = Mesh(mesh.devices.reshape(8, 4, mesh.shape["tp"]), ("sp_0", "sp_1", "tp"))
    in_specs = (
        P(SP, "tp"),
        P("tp", SP),
        P("tp", SP),
        P("tp", SP),
        P("tp", SP),
        P("tp", None),
        P(),
        P(SP, None),
        P(SP, None),
        P(SP, None, "tp"),
        P(SP, None, "tp"),
        P(SP, "tp", None),
    )
    out_specs = P(SP, "tp")
    return jax.shard_map(
        shards, mesh=finer, in_specs=in_specs, out_specs=out_specs, check_vma=False
    )
```

profile of v0, /device:TPU:24, one launch (start us, length us, event | category | flops | bytes accessed | tf_op | source)
XLA Modules:
  0.0 361.6 jit_solution(1007863958048043251)
XLA Ops:
  6.5 14.3 %all_gather.21 = bf16[128,1024]{1,0:T(8,128)(2,1)} all-gather(bf16[128,256]{1,0:T(8,128)(2,1)} %param.18), channel_id=1, replica_groups=mesh['sp_0'=8,'sp_1'=4,'tp'=16] {'sp_1'}, dimensions={1}, use_global_device_ids=true | all-gather | bytes 327680 | tf_op jit(solution)/shard_map/all_gather | solution.py:16
  20.9 13.2 %all_gather.25 = bf16[128,1024]{1,0:T(8,128)(2,1)} all-gather(bf16[128,256]{1,0:T(8,128)(2,1)} %param.19), channel_id=1, replica_groups=mesh['sp_0'=8,'sp_1'=4,'tp'=16] {'sp_1'}, dimensions={1}, use_global_device_ids=true | all-gather | bytes 327680 | tf_op jit(solution)/shard_map/all_gather | solution.py:16
  34.2 10.6 %all_gather.23 = f32[2,1024]{1,0:T(2,128)S(1)} all-gather(f32[2,256]{1,0:T(2,128)} %param.20), channel_id=1, replica_groups=mesh['sp_0'=8,'sp_1'=4,'tp'=16] {'sp_1'}, dimensions={1}, use_global_device_ids=true | all-gather | bytes 10240 | tf_op jit(solution)/shard_map/all_gather | solution.py:16
  44.8 31.0 %all_gather.24 = f32[2,8192]{1,0:T(2,128)S(1)} all-gather(f32[2,1024]{1,0:T(2,128)S(1)} %all_gather.23), channel_id=1, replica_groups=mesh['sp_0'=8,'sp_1'=4,'tp'=16] {'sp_0'}, dimensions={1}, use_global_device_ids=true | all-gather | bytes 73728 | tf_op jit(solution)/shard_map/all_gather | solution.py:16
  75.7 36.7 %all-gather.6.cloned.1.call-done = bf16[128,8192]{1,0:T(8,128)(2,1)} async-done(((bf16[128,1024]{1,0:T(8,128)(2,1)}), bf16[128,8192]{1,0:T(8,128)(2,1)}) %all-gather.6.cloned.1.call-update) | async-done | bytes 2097168 | tf_op jit(solution)/shard_map/all_gather | solution.py:16
  112.5 4.2 %while.18 = (s32[]{:T(128)}, f32[2,256]{1,0:T(2,128)S(1)}, f32[2,256]{1,0:T(2,128)S(1)}, f32[2,64,256]{2,1,0:T(8,128)S(1)}, s32[]{:T(128)}, /*index=5*/bf16[128,...) while((s32[]{:T(128)}, f32[2,256]{1,0:T(2,128)S(1)}, ...), condition=%wide.region_5.6_spmd.clone, body=%wide.region_0.5_spmd.clone.sunk | while | flops 139266304 | bytes 8788313 | solution.py:113
  112.5 3.8 %conditional.3 = ((f32[2,256]{1,0:T(2,128)S(1)}, f32[2,256]{1,0:T(2,128)S(1)}, f32[2,64,256]{2,1,0:T(8,128)S(1)})) conditional(s32[]{:T(128)} %convert_element_type.119, (f32[2,256]{1,0:T(2,128)S(1)}, f32[2,256]{1,0:T(2,128)S(1)}, f32[2,64,256]{2,1,0:T(8,128)S(1)}) %tuple.55, (s32[]{:T(128)}, s32[]{:T(128)}, bf16[128,8192]{1,0:T(8,128)(2,1)}, ...), branch_computations={%region_1.0_spmd, %region_2.4_spmd} | conditional | flops 139266304 | bytes 8787026 | solution.py:106
  113.9 1.6 fusion.26
  118.4 7.4 %all-to-all-start = ((bf16[16,256,128]{2,1,0:T(8,128)(2,1)}), bf16[16,256,128]{2,1,0:T(8,128)(2,1)S(1)}, u32[]{:S(2)}, u32[]{:S(2)}) async-start(bf16[16,256,128]{2,1,0:T(8,128)(2,1)} %bitcast.60), calls=%async_computation | async-start | bytes 2097152 | tf_op jit(solution)/shard_map/all_to_all | solution.py:27
  128.4 23.6 %all-to-all-done = bf16[16,256,128]{2,1,0:T(8,128)(2,1)S(1)} async-done(((bf16[16,256,128]{2,1,0:T(8,128)(2,1)}), bf16[16,256,128]{2,1,0:T(8,128)(2,1)S(1)}, u32[]{:S(2)}, u32[]{:S(2)}) %all-to-all-start) | async-done | bytes 1048608 | tf_op jit(solution)/shard_map/all_to_all | solution.py:27
  152.9 5.2 %all-to-all-start.1 = ((f32[16,1,256]{2,1,0:T(1,128)}), f32[16,1,256]{2,1,0:T(1,128)S(1)}, u32[]{:S(2)}, u32[]{:S(2)}) async-start(f32[16,1,256]{2,1,0:T(1,128)} %broadcast_in_dim.101), calls=%async_computation.1 | async-start | bytes 32768 | tf_op jit(solution)/shard_map/all_to_all | solution.py:33
  159.1 3.6 all-to-all-done.1
  162.8 2.0 gather_fusion
  165.1 44.1 %all_to_all.26 = bf16[32,20,128]{2,1,0:T(8,128)(2,1)} all-to-all(bf16[32,20,128]{2,1,0:T(8,128)(2,1)S(1)} %select_select_fusion), channel_id=1, replica_groups=mesh['sp_0'=8,'sp_1'=4,'tp'=16] {'sp_0','sp_1'}, dimensions={0} | all-to-all | bytes 327680 | tf_op jit(solution)/shard_map/all_to_all | solution.py:151
  209.2 39.2 %all-gather.8.cloned.1.call-done = bf16[32,20,2048]{2,1,0:T(8,128)(2,1)} async-done(((bf16[32,20,128]{2,1,0:T(8,128)(2,1)}), bf16[32,20,2048]{2,1,0:T(8,128)(2,1)}) %all-gather.8.cloned.1.call-update) | async-done | bytes 2621456 | tf_op jit(solution)/shard_map/all_gather | solution.py:150
  248.5 5.2 %reshape.235 = bf16[640,2048]{1,0:T(8,128)(2,1)} reshape(bf16[32,20,2048]{2,1,0:T(8,128)(2,1)} %all-gather.8.cloned.1.call-done) | data formatting | bytes 5242880 | tf_op jit(solution)/shard_map/reshape | solution.py:164
  253.7 2.7 fusion.12
  258.3 2.2 copy.94
  260.5 6.4 %all-to-all-start.3 = ((bf16[16,32,20,128]{3,1,2,0:T(8,128)(2,1)}), bf16[16,32,20,128]{3,1,2,0:T(8,128)(2,1)}, u32[]{:S(2)}, u32[]{:S(2)}) async-start(bf16[16,32,20,128]{3,1,2,0:T(8,128)(2,1)} %bitcast.62), calls=%async_computation.3 | async-start | bytes 5242880 | tf_op jit(solution)/shard_map/all_to_all | solution.py:27
  267.8 59.1 %all-to-all-done.3 = bf16[16,32,20,128]{3,1,2,0:T(8,128)(2,1)} async-done(((bf16[16,32,20,128]{3,1,2,0:T(8,128)(2,1)}), bf16[16,32,20,128]{3,1,2,0:T(8,128)(2,1)}, u32[]{:S(2)}, u32[]{:S(2)}) %all-to-all-start.3) | async-done | bytes 2621472 | tf_op jit(solution)/shard_map/all_to_all | solution.py:27
  326.9 2.1 reduce_sum.94
  329.8 9.9 %all-to-all-start.4 = ((bf16[32,20,128]{2,1,0:T(8,128)(2,1)}), bf16[32,20,128]{2,1,0:T(8,128)(2,1)S(1)}, u32[]{:S(2)}, u32[]{:S(2)}) async-start(bf16[32,20,128]{2,1,0:T(8,128)(2,1)} %copy.80), calls=%async_computation.4 | async-start | bytes 393216 | tf_op jit(solution)/shard_map/all_to_all | solution.py:172
  339.7 11.8 %all-to-all-done.4 = bf16[32,20,128]{2,1,0:T(8,128)(2,1)S(1)} async-done(((bf16[32,20,128]{2,1,0:T(8,128)(2,1)}), bf16[32,20,128]{2,1,0:T(8,128)(2,1)S(1)}, u32[]{:S(2)}, u32[]{:S(2)}) %all-to-all-start.4) | async-done | bytes 163872 | tf_op jit(solution)/shard_map/all_to_all | solution.py:172
  353.0 1.5 multiply_reduce_fusion
  (97 shorter events, 14.3 us)
Async XLA Ops:
  6.5 250.9 %copy-start = (bf16[1,256,2048]{2,1,0:T(8,128)(2,1)S(1)}, bf16[1,256,2048]{2,1,0:T(8,128)(2,1)}, u32[]{:S(2)}) copy-start(bf16[1,256,2048]{2,1,0:T(8,128)(2,1)} %param.27) | copy-start | bytes 3145732
  6.5 69.2 %all-gather.4.cloned.1.call-start = ((), (), s32[]{:S(2)}) async-start(), calls=%async_computation.5 | async-start | bytes 2359296 | tf_op jit(solution)/shard_map/all_gather | solution.py:16
  20.9 91.5 %all-gather.6.cloned.1.call-start = ((), (), s32[]{:S(2)}) async-start(), calls=%async_computation.6 | async-start | bytes 2359296 | tf_op jit(solution)/shard_map/all_gather | solution.py:16
  112.4 4.2 %copy-start.2 = (bf16[128,2048]{1,0:T(8,128)(2,1)S(1)}, bf16[128,2048]{1,0:T(8,128)(2,1)}, u32[]{:S(2)}) copy-start(bf16[128,2048]{1,0:T(8,128)(2,1)} %param.21) | copy-start | bytes 1572868
  117.2 8.7 %copy-start.4 = (s32[256,2]{0,1:T(2,128)S(1)}, s32[256,2]{0,1:T(2,128)}, u32[]{:S(2)}) copy-start(s32[256,2]{0,1:T(2,128)} %param.23) | copy-start | bytes 6148
  118.4 33.7 %copy-start.3 = (bf16[256,128]{1,0:T(8,128)(2,1)S(1)}, bf16[256,128]{1,0:T(8,128)(2,1)}, u32[]{:S(2)}) copy-start(bf16[256,128]{1,0:T(8,128)(2,1)} %param.16) | copy-start | bytes 196612
  118.4 33.6 %all-to-all-start = ((bf16[16,256,128]{2,1,0:T(8,128)(2,1)}), bf16[16,256,128]{2,1,0:T(8,128)(2,1)S(1)}, u32[]{:S(2)}, u32[]{:S(2)}) async-start(bf16[16,256,128]{2,1,0:T(8,128)(2,1)} %bitcast.60), calls=%async_computation | async-start | bytes 2097152 | tf_op jit(solution)/shard_map/all_to_all | solution.py:27
  152.9 9.7 %all-to-all-start.1 = ((f32[16,1,256]{2,1,0:T(1,128)}), f32[16,1,256]{2,1,0:T(1,128)S(1)}, u32[]{:S(2)}, u32[]{:S(2)}) async-start(f32[16,1,256]{2,1,0:T(1,128)} %broadcast_in_dim.101), calls=%async_computation.1 | async-start | bytes 32768 | tf_op jit(solution)/shard_map/all_to_all | solution.py:33
  158.1 90.4 %all-gather.8.cloned.1.call-start = ((), (), s32[]{:S(2)}) async-start(), calls=%async_computation.7 | async-start | bytes 3342336 | tf_op jit(solution)/shard_map/all_gather | solution.py:150
  209.2 44.4 %copy-start.6 = (bf16[1,2048,256]{2,1,0:T(8,128)(2,1)S(1)}, bf16[1,2048,256]{2,1,0:T(8,128)(2,1)}, u32[]{:S(2)}) copy-start(bf16[1,2048,256]{2,1,0:T(8,128)(2,1)} %param.25) | copy-start | bytes 3145732
  253.7 2.8 copy-start.1
  253.7 2.8 copy-start.7
  260.5 7.2 %copy-start.5 = (f32[256,2]{0,1:T(2,128)S(1)}, f32[256,2]{0,1:T(2,128)}, u32[]{:S(2)}) copy-start(f32[256,2]{0,1:T(2,128)} %param.24) | copy-start | bytes 6148
  260.5 66.5 %all-to-all-start.3 = ((bf16[16,32,20,128]{3,1,2,0:T(8,128)(2,1)}), bf16[16,32,20,128]{3,1,2,0:T(8,128)(2,1)}, u32[]{:S(2)}, u32[]{:S(2)}) async-start(bf16[16,32,20,128]{3,1,2,0:T(8,128)(2,1)} %bitcast.62), calls=%async_computation.3 | async-start | bytes 5242880 | tf_op jit(solution)/shard_map/all_to_all | solution.py:27
  329.8 21.8 %all-to-all-start.4 = ((bf16[32,20,128]{2,1,0:T(8,128)(2,1)}), bf16[32,20,128]{2,1,0:T(8,128)(2,1)S(1)}, u32[]{:S(2)}, u32[]{:S(2)}) async-start(bf16[32,20,128]{2,1,0:T(8,128)(2,1)} %copy.80), calls=%async_computation.4 | async-start | bytes 393216 | tf_op jit(solution)/shard_map/all_to_all | solution.py:172
Sparse Core Ops, SparseCore 0:
  21.0 47.3 all-gather.3
  70.5 41.8 all-gather.5
  209.3 39.0 all-gather.7
where the time goes:
time: 363 us; the launch traced here: 362 us
  waiting for transfers between devices  174 us (48%)
  blocking collectives  113 us (31%)
  starting transfers between devices  29 us (8%)
  local copies, waits for them, and re-layouts  17.1 us (5%)
  between operations  13.4 us (4%)
  other arithmetic  7.3 us (2%)
  matrix products  6.94 us (2%)
    all_to_all x2, waiting for transfers between devices, sum_at_owner(): lax.all_to_all(cut_along(shard, dim, peers), axis, 0, 0, tiled=True)  82.8 us
    all_gather x4, blocking collectives, gathered_by_axis(): out = lax.all_gather(out, axes[number], axis=dim, tiled=True)  69.1 us
    all_to_all x1, blocking collectives, shards(): lax.all_to_all(taken_rows.reshape(sp_count, capacity, normed.shape[1]), S...  44.1 us
    all_gather x1, waiting for transfers between devices, shards(): lax.all_gather(lax.all_to_all(taken_rows.reshape(sp_count, capacity, norm...  39.2 us
    all_gather x2, waiting for transfers between devices, gathered_by_axis(): out = lax.all_gather(out, axes[number], axis=dim, tiled=True)  36.7 us
    all_to_all x2, starting transfers between devices, sum_at_owner(): lax.all_to_all(cut_along(shard, dim, peers), axis, 0, 0, tiled=True)  13.8 us
    all_to_all x1, waiting for transfers between devices, shards(): lax.all_to_all(summed.astype(jnp.bfloat16), SP, split_axis=0, concat_axis...  11.8 us
    all_to_all x1, starting transfers between devices, shards(): lax.all_to_all(summed.astype(jnp.bfloat16), SP, split_axis=0, concat_axis...  9.92 us
  transfers between devices with their start and end apart: 7, of which 6 were waited for; matrix products, arithmetic and copies ran while one was open for 1% of the time, Pallas kernels for 0%

commit v1 on v0

--- a/solution.py
+++ b/solution.py
@@ -147,18 +147,29 @@
     normed = (local_rows * row_scale[:, None] * local_gain[None, :]).astype(jnp.bfloat16)
     taken_rows = jnp.take(normed, source_row, axis=0)
     taken_rows = jnp.where(filled[:, None], taken_rows, jnp.zeros((), normed.dtype))
-    arrived = lax.all_gather(
-        lax.all_to_all(
-            taken_rows.reshape(sp_count, capacity, normed.shape[1]),
-            SP,
-            split_axis=0,
-            concat_axis=0,
-            tiled=True,
-        ),
-        "tp",
-        axis=2,
+    value = lax.all_to_all(
+        taken_rows.reshape(sp_count, capacity, normed.shape[1]),
+        SP,
+        split_axis=0,
+        concat_axis=0,
         tiled=True,
     )
+    ways, here, step = (lax.axis_size("tp"), lax.axis_index("tp"), value.shape[2])
+    lengths = [n * ways if d == 2 else n for d, n in enumerate(value.shape)]
+    arrived = lax.dynamic_update_slice_in_dim(
+        jnp.zeros(lengths, value.dtype), value, here * step, axis=2
+    )
+    going_up = going_down = value
+    for far in range(1, ways // 2 + 1):
+        going_up = lax.ppermute(going_up, "tp", [(d, (d + 1) % ways) for d in range(ways)])
+        arrived = lax.dynamic_update_slice_in_dim(
+            arrived, going_up, (here - far) % ways * step, axis=2
+        )
+        if 2 * far < ways:
+            going_down = lax.ppermute(going_down, "tp", [(d, (d - 1) % ways) for d in range(ways)])
+            arrived = lax.dynamic_update_slice_in_dim(
+                arrived, going_down, (here + far) % ways * step, axis=2
+            )
     source_count = arrived.shape[0]
     slot_count = arrived.shape[1]
     flat_rows = arrived.reshape(source_count * slot_count, model_width)

time: 363 us -> 370 us (1.019)
  waiting for transfers between devices: 174 us -> 144 us
  starting transfers between devices: 29 us -> 52.9 us
  local copies, waits for them, and re-layouts: 17.1 us -> 30.7 us
    all_gather x1 -> x0, waiting for transfers between devices: 39.2 us -> none  [shards(): lax.all_gather(lax.all_to_all(taken_rows.reshape(sp_count, capacity, norm...]
    ppermute x0 -> x15, starting transfers between devices: none -> 21.1 us  [the longest x8 14.8 us: shards(): lax.ppermute(going_up, 'tp', [(d, (d + 1) % ways) for d in range(ways)])]
    dynamic_update_slice x0 -> x16, local copies, waits for them, and re-layouts: none -> 11.6 us  [the longest x8 5.75 us: shards(): lax.dynamic_update_slice_in_dim(arrived, going_up, (here - far) % ways *...]
    all_to_all x2, starting transfers between devices: 13.8 us -> 22.6 us  [sum_at_owner(): lax.all_to_all(cut_along(shard, dim, peers), axis, 0, 0, tiled=True)]
    ppermute x0 -> x15, waiting for transfers between devices: none -> 8.61 us  [the longest x8 8.59 us: shards(): lax.ppermute(going_up, 'tp', [(d, (d + 1) % ways) for d in range(ways)])]
    all_to_all x1, starting transfers between devices: 9.92 us -> 3.86 us  [shards(): lax.all_to_all(summed.astype(jnp.bfloat16), SP, split_axis=0, concat_axis...]
  transfers between devices with their start and end apart: 7 -> 21, of which waited for: 6 -> 11; matrix products, arithmetic and copies ran while one was open for 1% -> 5% of each run, Pallas kernels for 0% -> 0%
where the time goes in v1:
time: 370 us; the launch traced here: 369 us
  waiting for transfers between devices  144 us (39%)
  blocking collectives  113 us (31%)
  starting transfers between devices  52.9 us (14%)
  local copies, waits for them, and re-layouts  30.7 us (8%)
  between operations  13.8 us (4%)
  other arithmetic  7.3 us (2%)
  matrix products  6.94 us (2%)
    all_to_all x2, waiting for transfers between devices, sum_at_owner(): lax.all_to_all(cut_along(shard, dim, peers), axis, 0, 0, tiled=True)  82.8 us
    all_gather x4, blocking collectives, gathered_by_axis(): out = lax.all_gather(out, axes[number], axis=dim, tiled=True)  69.1 us
    all_to_all x1, blocking collectives, shards(): lax.all_to_all(taken_rows.reshape(sp_count, capacity, normed.shape[1]), S...  44 us
    all_gather x2, waiting for transfers between devices, gathered_by_axis(): out = lax.all_gather(out, axes[number], axis=dim, tiled=True)  36.7 us
    all_to_all x2, starting transfers between devices, sum_at_owner(): lax.all_to_all(cut_along(shard, dim, peers), axis, 0, 0, tiled=True)  22.6 us
    ppermute x8, starting transfers between devices, shards(): lax.ppermute(going_up, 'tp', [(d, (d + 1) % ways) for d in range(ways)])  14.8 us
    all_to_all x1, waiting for transfers between devices, shards(): lax.all_to_all(summed.astype(jnp.bfloat16), SP, split_axis=0, concat_axis...  12.3 us
    ppermute x8, waiting for transfers between devices, shards(): lax.ppermute(going_up, 'tp', [(d, (d + 1) % ways) for d in range(ways)])  8.59 us
  transfers between devices with their start and end apart: 21, of which 11 were waited for; matrix products, arithmetic and copies ran while one was open for 5% of the time, Pallas kernels for 0%

profile of v1, /device:TPU:24, one launch (start us, length us, event | category | flops | bytes accessed | tf_op | source)
XLA Modules:
  0.0 369.1 jit_solution(2559893279427847043)
XLA Ops:
  6.5 14.3 %all_gather.18 = bf16[128,1024]{1,0:T(8,128)(2,1)} all-gather(bf16[128,256]{1,0:T(8,128)(2,1)} %param.18), channel_id=1, replica_groups=mesh['sp_0'=8,'sp_1'=4,'tp'=16] {'sp_1'}, dimensions={1}, use_global_device_ids=true | all-gather | bytes 327680 | tf_op jit(solution)/shard_map/all_gather | solution.py:16
  20.9 13.2 %all_gather.22 = bf16[128,1024]{1,0:T(8,128)(2,1)} all-gather(bf16[128,256]{1,0:T(8,128)(2,1)} %param.19), channel_id=1, replica_groups=mesh['sp_0'=8,'sp_1'=4,'tp'=16] {'sp_1'}, dimensions={1}, use_global_device_ids=true | all-gather | bytes 327680 | tf_op jit(solution)/shard_map/all_gather | solution.py:16
  34.2 10.6 %all_gather.20 = f32[2,1024]{1,0:T(2,128)S(1)} all-gather(f32[2,256]{1,0:T(2,128)} %param.20), channel_id=1, replica_groups=mesh['sp_0'=8,'sp_1'=4,'tp'=16] {'sp_1'}, dimensions={1}, use_global_device_ids=true | all-gather | bytes 10240 | tf_op jit(solution)/shard_map/all_gather | solution.py:16
  44.8 31.0 %all_gather.21 = f32[2,8192]{1,0:T(2,128)S(1)} all-gather(f32[2,1024]{1,0:T(2,128)S(1)} %all_gather.20), channel_id=1, replica_groups=mesh['sp_0'=8,'sp_1'=4,'tp'=16] {'sp_0'}, dimensions={1}, use_global_device_ids=true | all-gather | bytes 73728 | tf_op jit(solution)/shard_map/all_gather | solution.py:16
  75.8 36.7 %all-gather.5.cloned.1.call-done = bf16[128,8192]{1,0:T(8,128)(2,1)} async-done(((bf16[128,1024]{1,0:T(8,128)(2,1)}), bf16[128,8192]{1,0:T(8,128)(2,1)}) %all-gather.5.cloned.1.call-update) | async-done | bytes 2097168 | tf_op jit(solution)/shard_map/all_gather | solution.py:16
  112.5 4.2 %while.18 = (s32[]{:T(128)}, f32[2,256]{1,0:T(2,128)S(1)}, f32[2,256]{1,0:T(2,128)S(1)}, f32[2,64,256]{2,1,0:T(8,128)S(1)}, s32[]{:T(128)}, /*index=5*/bf16[128,...) while((s32[]{:T(128)}, f32[2,256]{1,0:T(2,128)S(1)}, ...), condition=%wide.region_5.6_spmd.clone, body=%wide.region_0.5_spmd.clone.sunk | while | flops 139266304 | bytes 8788313 | solution.py:113
  112.5 3.8 %conditional.3 = ((f32[2,256]{1,0:T(2,128)S(1)}, f32[2,256]{1,0:T(2,128)S(1)}, f32[2,64,256]{2,1,0:T(8,128)S(1)})) conditional(s32[]{:T(128)} %convert_element_type.119, (f32[2,256]{1,0:T(2,128)S(1)}, f32[2,256]{1,0:T(2,128)S(1)}, f32[2,64,256]{2,1,0:T(8,128)S(1)}) %tuple.55, (s32[]{:T(128)}, s32[]{:T(128)}, bf16[128,8192]{1,0:T(8,128)(2,1)}, ...), branch_computations={%region_1.0_spmd, %region_2.4_spmd} | conditional | flops 139266304 | bytes 8787026 | solution.py:106
  118.4 7.3 %all-to-all-start = ((bf16[16,256,128]{2,1,0:T(8,128)(2,1)}), bf16[16,256,128]{2,1,0:T(8,128)(2,1)S(1)}, u32[]{:S(2)}, u32[]{:S(2)}) async-start(bf16[16,256,128]{2,1,0:T(8,128)(2,1)} %bitcast.62), calls=%async_computation | async-start | bytes 2097152 | tf_op jit(solution)/shard_map/all_to_all | solution.py:27
  128.3 23.6 %all-to-all-done = bf16[16,256,128]{2,1,0:T(8,128)(2,1)S(1)} async-done(((bf16[16,256,128]{2,1,0:T(8,128)(2,1)}), bf16[16,256,128]{2,1,0:T(8,128)(2,1)S(1)}, u32[]{:S(2)}, u32[]{:S(2)}) %all-to-all-start) | async-done | bytes 1048608 | tf_op jit(solution)/shard_map/all_to_all | solution.py:27
  152.8 5.2 %all-to-all-start.1 = ((f32[16,1,256]{2,1,0:T(1,128)}), f32[16,1,256]{2,1,0:T(1,128)S(1)}, u32[]{:S(2)}, u32[]{:S(2)}) async-start(f32[16,1,256]{2,1,0:T(1,128)} %broadcast_in_dim.105), calls=%async_computation.1 | async-start | bytes 32768 | tf_op jit(solution)/shard_map/all_to_all | solution.py:33
  158.9 3.6 all-to-all-done.1
  165.0 44.0 %all_to_all.26 = bf16[32,20,128]{2,1,0:T(8,128)(2,1)S(1)} all-to-all(bf16[32,20,128]{2,1,0:T(8,128)(2,1)S(1)} %select_select_fusion), channel_id=1, replica_groups=mesh['sp_0'=8,'sp_1'=4,'tp'=16] {'sp_0','sp_1'}, dimensions={0} | all-to-all | bytes 327680 | tf_op jit(solution)/shard_map/all_to_all | solution.py:150
  210.7 2.0 broadcast_in_dim.99
  234.4 3.1 collective-permute-start.10
  239.5 4.3 %collective-permute-start.12 = (bf16[32,20,128]{2,1,0:T(8,128)(2,1)S(1)}, bf16[32,20,128]{2,1,0:T(8,128)(2,1)S(1)}, u32[]{:S(2)}, u32[]{:S(2)}) collective-permute-start(bf16[32,20,128]{2,1,0:T(8,128)(2,1)S(1)} %collective-permute-done.10), channel_id=1, source_target_pairs={{0,1},{1,2},{2,3},{3,4},{4,5},{5,6},{6,7},{7,8},{8,9},{9,10},{10,1... | collective-permute-start | bytes 491528 | tf_op jit(solution)/shard_map/ppermute | solution.py:164
  245.3 4.8 %collective-permute-start.14 = (bf16[32,20,128]{2,1,0:T(8,128)(2,1)S(1)}, bf16[32,20,128]{2,1,0:T(8,128)(2,1)S(1)}, u32[]{:S(2)}, u32[]{:S(2)}) collective-permute-start(bf16[32,20,128]{2,1,0:T(8,128)(2,1)S(1)} %collective-permute-done.12), channel_id=1, source_target_pairs={{0,1},{1,2},{2,3},{3,4},{4,5},{5,6},{6,7},{7,8},{8,9},{9,10},{10,1... | collective-permute-start | bytes 491528 | tf_op jit(solution)/shard_map/ppermute | solution.py:164
  252.3 5.2 %reshape.235 = bf16[640,2048]{1,0:T(8,128)(2,1)} reshape(bf16[32,20,2048]{2,1,0:T(8,128)(2,1)} %constant_dynamic-update-slice_fusion) | data formatting | bytes 5242880 | tf_op jit(solution)/shard_map/reshape | solution.py:175
  257.5 2.7 fusion.12
  262.1 2.2 copy.94
  264.3 15.4 %all-to-all-start.3 = ((bf16[16,32,20,128]{3,1,2,0:T(8,128)(2,1)}), bf16[16,32,20,128]{3,1,2,0:T(8,128)(2,1)}, u32[]{:S(2)}, u32[]{:S(2)}) async-start(bf16[16,32,20,128]{3,1,2,0:T(8,128)(2,1)} %bitcast.64), calls=%async_computation.3 | async-start | bytes 5242880 | tf_op jit(solution)/shard_map/all_to_all | solution.py:27
  280.6 59.1 %all-to-all-done.3 = bf16[16,32,20,128]{3,1,2,0:T(8,128)(2,1)} async-done(((bf16[16,32,20,128]{3,1,2,0:T(8,128)(2,1)}), bf16[16,32,20,128]{3,1,2,0:T(8,128)(2,1)}, u32[]{:S(2)}, u32[]{:S(2)}) %all-to-all-start.3) | async-done | bytes 2621472 | tf_op jit(solution)/shard_map/all_to_all | solution.py:27
  339.7 2.1 reduce_sum.94
  342.6 3.9 %all-to-all-start.4 = ((bf16[32,20,128]{2,1,0:T(8,128)(2,1)}), bf16[32,20,128]{2,1,0:T(8,128)(2,1)S(1)}, u32[]{:S(2)}, u32[]{:S(2)}) async-start(bf16[32,20,128]{2,1,0:T(8,128)(2,1)} %copy.80), calls=%async_computation.4 | async-start | bytes 393216 | tf_op jit(solution)/shard_map/all_to_all | solution.py:183
  346.5 12.3 %all-to-all-done.4 = bf16[32,20,128]{2,1,0:T(8,128)(2,1)S(1)} async-done(((bf16[32,20,128]{2,1,0:T(8,128)(2,1)}), bf16[32,20,128]{2,1,0:T(8,128)(2,1)S(1)}, u32[]{:S(2)}, u32[]{:S(2)}) %all-to-all-start.4) | async-done | bytes 163872 | tf_op jit(solution)/shard_map/all_to_all | solution.py:183
  (141 shorter events, 48.3 us)
Async XLA Ops:
  6.5 254.7 %copy-start = (bf16[1,256,2048]{2,1,0:T(8,128)(2,1)S(1)}, bf16[1,256,2048]{2,1,0:T(8,128)(2,1)}, u32[]{:S(2)}) copy-start(bf16[1,256,2048]{2,1,0:T(8,128)(2,1)} %param.27) | copy-start | bytes 3145732
  6.5 69.2 %all-gather.3.cloned.1.call-start = ((), (), s32[]{:S(2)}) async-start(), calls=%async_computation.5 | async-start | bytes 2359296 | tf_op jit(solution)/shard_map/all_gather | solution.py:16
  20.9 91.5 %all-gather.5.cloned.1.call-start = ((), (), s32[]{:S(2)}) async-start(), calls=%async_computation.6 | async-start | bytes 2359296 | tf_op jit(solution)/shard_map/all_gather | solution.py:16
  117.2 34.9 %copy-start.3 = (bf16[256,128]{1,0:T(8,128)(2,1)S(1)}, bf16[256,128]{1,0:T(8,128)(2,1)}, u32[]{:S(2)}) copy-start(bf16[256,128]{1,0:T(8,128)(2,1)} %param.16) | copy-start | bytes 196612
  118.4 33.5 %all-to-all-start = ((bf16[16,256,128]{2,1,0:T(8,128)(2,1)}), bf16[16,256,128]{2,1,0:T(8,128)(2,1)S(1)}, u32[]{:S(2)}, u32[]{:S(2)}) async-start(bf16[16,256,128]{2,1,0:T(8,128)(2,1)} %bitcast.62), calls=%async_computation | async-start | bytes 2097152 | tf_op jit(solution)/shard_map/all_to_all | solution.py:27
  152.8 9.7 %all-to-all-start.1 = ((f32[16,1,256]{2,1,0:T(1,128)}), f32[16,1,256]{2,1,0:T(1,128)S(1)}, u32[]{:S(2)}, u32[]{:S(2)}) async-start(f32[16,1,256]{2,1,0:T(1,128)} %broadcast_in_dim.105), calls=%async_computation.1 | async-start | bytes 32768 | tf_op jit(solution)/shard_map/all_to_all | solution.py:33
  209.0 5.1 %collective-permute-start = (bf16[32,20,128]{2,1,0:T(8,128)(2,1)S(1)}, bf16[32,20,128]{2,1,0:T(8,128)(2,1)S(1)}, u32[]{:S(2)}, u32[]{:S(2)}) collective-permute-start(bf16[32,20,128]{2,1,0:T(8,128)(2,1)S(1)} %all_to_all.26), channel_id=1, source_target_pairs={{0,1},{1,2},{2,3},{3,4},{4,5},{5,6},{6,7},{7,8},{8,9},{9,10},{10,1... | collective-permute-start | bytes 491528 | tf_op jit(solution)/shard_map/ppermute | solution.py:164
  209.0 5.1 %collective-permute-start.1 = (bf16[32,20,128]{2,1,0:T(8,128)(2,1)S(1)}, bf16[32,20,128]{2,1,0:T(8,128)(2,1)S(1)}, u32[]{:S(2)}, u32[]{:S(2)}) collective-permute-start(bf16[32,20,128]{2,1,0:T(8,128)(2,1)S(1)} %all_to_all.26), channel_id=1, source_target_pairs={{0,15},{1,0},{2,1},{3,2},{4,3},{5,4},{6,5},{7,6},{8,7},{9,8},{10,9... | collective-permute-start | bytes 491528 | tf_op jit(solution)/shard_map/ppermute | solution.py:169
  214.1 5.1 %collective-permute-start.2 = (bf16[32,20,128]{2,1,0:T(8,128)(2,1)S(1)}, bf16[32,20,128]{2,1,0:T(8,128)(2,1)S(1)}, u32[]{:S(2)}, u32[]{:S(2)}) collective-permute-start(bf16[32,20,128]{2,1,0:T(8,128)(2,1)S(1)} %collective-permute-done), channel_id=1, source_target_pairs={{0,1},{1,2},{2,3},{3,4},{4,5},{5,6},{6,7},{7,8},{8,9},{9,10},{10,1... | collective-permute-start | bytes 491528 | tf_op jit(solution)/shard_map/ppermute | solution.py:164
  214.1 5.1 %collective-permute-start.3 = (bf16[32,20,128]{2,1,0:T(8,128)(2,1)S(1)}, bf16[32,20,128]{2,1,0:T(8,128)(2,1)S(1)}, u32[]{:S(2)}, u32[]{:S(2)}) collective-permute-start(bf16[32,20,128]{2,1,0:T(8,128)(2,1)S(1)} %collective-permute-done.1), channel_id=1, source_target_pairs={{0,15},{1,0},{2,1},{3,2},{4,3},{5,4},{6,5},{7,6},{8,7},{9,8},{10,9... | collective-permute-start | bytes 491528 | tf_op jit(solution)/shard_map/ppermute | solution.py:169
  219.2 5.1 %collective-permute-start.4 = (bf16[32,20,128]{2,1,0:T(8,128)(2,1)S(1)}, bf16[32,20,128]{2,1,0:T(8,128)(2,1)S(1)}, u32[]{:S(2)}, u32[]{:S(2)}) collective-permute-start(bf16[32,20,128]{2,1,0:T(8,128)(2,1)S(1)} %collective-permute-done.2), channel_id=1, source_target_pairs={{0,1},{1,2},{2,3},{3,4},{4,5},{5,6},{6,7},{7,8},{8,9},{9,10},{10,1... | collective-permute-start | bytes 491528 | tf_op jit(solution)/shard_map/ppermute | solution.py:164
  219.2 5.8 %collective-permute-start.5 = (bf16[32,20,128]{2,1,0:T(8,128)(2,1)S(1)}, bf16[32,20,128]{2,1,0:T(8,128)(2,1)S(1)}, u32[]{:S(2)}, u32[]{:S(2)}) collective-permute-start(bf16[32,20,128]{2,1,0:T(8,128)(2,1)S(1)} %collective-permute-done.3), channel_id=1, source_target_pairs={{0,15},{1,0},{2,1},{3,2},{4,3},{5,4},{6,5},{7,6},{8,7},{9,8},{10,9... | collective-permute-start | bytes 491528 | tf_op jit(solution)/shard_map/ppermute | solution.py:169
  224.2 5.1 %collective-permute-start.6 = (bf16[32,20,128]{2,1,0:T(8,128)(2,1)S(1)}, bf16[32,20,128]{2,1,0:T(8,128)(2,1)S(1)}, u32[]{:S(2)}, u32[]{:S(2)}) collective-permute-start(bf16[32,20,128]{2,1,0:T(8,128)(2,1)S(1)} %collective-permute-done.4), channel_id=1, source_target_pairs={{0,1},{1,2},{2,3},{3,4},{4,5},{5,6},{6,7},{7,8},{8,9},{9,10},{10,1... | collective-permute-start | bytes 491528 | tf_op jit(solution)/shard_map/ppermute | solution.py:164
  224.9 6.3 %collective-permute-start.7 = (bf16[32,20,128]{2,1,0:T(8,128)(2,1)S(1)}, bf16[32,20,128]{2,1,0:T(8,128)(2,1)S(1)}, u32[]{:S(2)}, u32[]{:S(2)}) collective-permute-start(bf16[32,20,128]{2,1,0:T(8,128)(2,1)S(1)} %collective-permute-done.5), channel_id=1, source_target_pairs={{0,15},{1,0},{2,1},{3,2},{4,3},{5,4},{6,5},{7,6},{8,7},{9,8},{10,9... | collective-permute-start | bytes 491528 | tf_op jit(solution)/shard_map/ppermute | solution.py:169
  229.3 5.1 %collective-permute-start.8 = (bf16[32,20,128]{2,1,0:T(8,128)(2,1)S(1)}, bf16[32,20,128]{2,1,0:T(8,128)(2,1)S(1)}, u32[]{:S(2)}, u32[]{:S(2)}) collective-permute-start(bf16[32,20,128]{2,1,0:T(8,128)(2,1)S(1)} %collective-permute-done.6), channel_id=1, source_target_pairs={{0,1},{1,2},{2,3},{3,4},{4,5},{5,6},{6,7},{7,8},{8,9},{9,10},{10,1... | collective-permute-start | bytes 491528 | tf_op jit(solution)/shard_map/ppermute | solution.py:164
  231.2 6.3 %collective-permute-start.9 = (bf16[32,20,128]{2,1,0:T(8,128)(2,1)S(1)}, bf16[32,20,128]{2,1,0:T(8,128)(2,1)S(1)}, u32[]{:S(2)}, u32[]{:S(2)}) collective-permute-start(bf16[32,20,128]{2,1,0:T(8,128)(2,1)S(1)} %collective-permute-done.7), channel_id=1, source_target_pairs={{0,15},{1,0},{2,1},{3,2},{4,3},{5,4},{6,5},{7,6},{8,7},{9,8},{10,9... | collective-permute-start | bytes 491528 | tf_op jit(solution)/shard_map/ppermute | solution.py:169
  234.4 5.1 %collective-permute-start.10 = (bf16[32,20,128]{2,1,0:T(8,128)(2,1)S(1)}, bf16[32,20,128]{2,1,0:T(8,128)(2,1)S(1)}, u32[]{:S(2)}, u32[]{:S(2)}) collective-permute-start(bf16[32,20,128]{2,1,0:T(8,128)(2,1)S(1)} %collective-permute-done.8), channel_id=1, source_target_pairs={{0,1},{1,2},{2,3},{3,4},{4,5},{5,6},{6,7},{7,8},{8,9},{9,10},{10,1... | collective-permute-start | bytes 491528 | tf_op jit(solution)/shard_map/ppermute | solution.py:164
  237.5 6.3 %collective-permute-start.11 = (bf16[32,20,128]{2,1,0:T(8,128)(2,1)S(1)}, bf16[32,20,128]{2,1,0:T(8,128)(2,1)S(1)}, u32[]{:S(2)}, u32[]{:S(2)}) collective-permute-start(bf16[32,20,128]{2,1,0:T(8,128)(2,1)S(1)} %collective-permute-done.9), channel_id=1, source_target_pairs={{0,15},{1,0},{2,1},{3,2},{4,3},{5,4},{6,5},{7,6},{8,7},{9,8},{10,9... | collective-permute-start | bytes 491528 | tf_op jit(solution)/shard_map/ppermute | solution.py:169
  239.5 5.8 %collective-permute-start.12 = (bf16[32,20,128]{2,1,0:T(8,128)(2,1)S(1)}, bf16[32,20,128]{2,1,0:T(8,128)(2,1)S(1)}, u32[]{:S(2)}, u32[]{:S(2)}) collective-permute-start(bf16[32,20,128]{2,1,0:T(8,128)(2,1)S(1)} %collective-permute-done.10), channel_id=1, source_target_pairs={{0,1},{1,2},{2,3},{3,4},{4,5},{5,6},{6,7},{7,8},{8,9},{9,10},{10,1... | collective-permute-start | bytes 491528 | tf_op jit(solution)/shard_map/ppermute | solution.py:164
  243.8 7.0 %collective-permute-start.13 = (bf16[32,20,128]{2,1,0:T(8,128)(2,1)S(1)}, bf16[32,20,128]{2,1,0:T(8,128)(2,1)S(1)}, u32[]{:S(2)}, u32[]{:S(2)}) collective-permute-start(bf16[32,20,128]{2,1,0:T(8,128)(2,1)S(1)} %collective-permute-done.11), channel_id=1, source_target_pairs={{0,15},{1,0},{2,1},{3,2},{4,3},{5,4},{6,5},{7,6},{8,7},{9,8},{10,9... | collective-permute-start | bytes 491528 | tf_op jit(solution)/shard_map/ppermute | solution.py:169
  245.3 6.3 %collective-permute-start.14 = (bf16[32,20,128]{2,1,0:T(8,128)(2,1)S(1)}, bf16[32,20,128]{2,1,0:T(8,128)(2,1)S(1)}, u32[]{:S(2)}, u32[]{:S(2)}) collective-permute-start(bf16[32,20,128]{2,1,0:T(8,128)(2,1)S(1)} %collective-permute-done.12), channel_id=1, source_target_pairs={{0,1},{1,2},{2,3},{3,4},{4,5},{5,6},{6,7},{7,8},{8,9},{9,10},{10,1... | collective-permute-start | bytes 491528 | tf_op jit(solution)/shard_map/ppermute | solution.py:164
  264.3 16.1 %copy-start.5 = (f32[256,2]{0,1:T(2,128)S(1)}, f32[256,2]{0,1:T(2,128)}, u32[]{:S(2)}) copy-start(f32[256,2]{0,1:T(2,128)} %param.24) | copy-start | bytes 6148
  264.3 75.4 %all-to-all-start.3 = ((bf16[16,32,20,128]{3,1,2,0:T(8,128)(2,1)}), bf16[16,32,20,128]{3,1,2,0:T(8,128)(2,1)}, u32[]{:S(2)}, u32[]{:S(2)}) async-start(bf16[16,32,20,128]{3,1,2,0:T(8,128)(2,1)} %bitcast.64), calls=%async_computation.3 | async-start | bytes 5242880 | tf_op jit(solution)/shard_map/all_to_all | solution.py:27
  342.6 16.2 %all-to-all-start.4 = ((bf16[32,20,128]{2,1,0:T(8,128)(2,1)}), bf16[32,20,128]{2,1,0:T(8,128)(2,1)S(1)}, u32[]{:S(2)}, u32[]{:S(2)}) async-start(bf16[32,20,128]{2,1,0:T(8,128)(2,1)} %copy.80), calls=%async_computation.4 | async-start | bytes 393216 | tf_op jit(solution)/shard_map/all_to_all | solution.py:183
  (5 other events, 24.7 us)
Sparse Core Ops, SparseCore 0:
  21.0 47.3 all-gather.2
  70.4 41.9 all-gather.4
